TPU v7x, 32 devices: a whole 2x2x4 slice. The times are simulated.
32 devices in a mesh: sp: 8 (over z, x), tp: 4 (over y, core).
Axes of the slice: x: 2, y: 2, z: 4, core: 2. Of those that a mesh axis runs over, the one named last changes fastest.
Arguments:
- layer_input: bfloat16 [1280, 4096], P('sp', 'tp'), may hold values from -24 to 24
- output_grad: bfloat16 [1280, 4096], P('sp', 'tp'), may hold values from -24 to 24
- query_weight: bfloat16 [4096, 2048], P(None, 'tp'), may hold values from -0.09375 to 0.09375
- key_weight: bfloat16 [4096, 1024], P(None, 'tp'), may hold values from -0.09375 to 0.09375
- value_weight: bfloat16 [4096, 1024], P(None, 'tp'), may hold values from -0.09375 to 0.09375
- out_weight: bfloat16 [2048, 4096], P('tp'), may hold values from -0.125 to 0.125
- sink_logit: float32 [16], P('tp'), may hold values from 3 to 7
Outputs:
- input_grad: bfloat16 [1280, 4096], P('sp', 'tp')
- query_weight_grad: float32 [4096, 2048], P('sp', 'tp')
- key_weight_grad: float32 [4096, 1024], P('sp', 'tp')
- value_weight_grad: float32 [4096, 1024], P('sp', 'tp')
- out_weight_grad: float32 [2048, 4096], P('tp', 'sp')
- sink_grad: float32 [16], P('tp')
All inputs are finite; a program needn't handle non-finite values.
Results may differ from a plain program's by a relative error of at most 0.015.
Values may be sent and summed in bfloat16 or wider, within the bound.
A program may use at most 192 MiB of HBM per device.

v0:
```python
import jax
import jax.numpy as jnp
from jax import lax
from jax.sharding import PartitionSpec as P

HEADS = 16
KV_HEADS = 8
HEAD = 128
WINDOW = 128


masked_score = -1e30


def extended(cells, sides, width):
    for axis, dim in sides:
        count = lax.axis_size(axis)
        ends = count - 1
        head = lax.slice_in_dim(cells, 0, width, axis=dim)
        tail = lax.slice_in_dim(cells, cells.shape[dim] - width, cells.shape[dim], axis=dim)
        cells = jnp.concatenate(
            [
                lax.ppermute(tail, axis, [(i, (i + 1) % count) for i in range(ends)]),
                cells,
                lax.ppermute(head, axis, [((i + 1) % count, i) for i in range(ends)]),
            ],
            axis=dim,
        )
    return cells


def passed_along(value, axis, steps):
    count = lax.axis_size(axis)
    initial, last = (max(0, -steps), min(count, count - steps))
    return lax.ppermute(value, axis, [(source, source + steps) for source in range(initial, last)])


def contract_rows(left, right):
    return lax.dot_general(
        left, right, (((0,), (0,)), ((), ())), preferred_element_type=jnp.float32
    )


def contract_cols(left, right):
    return lax.dot_general(
        left, right, (((1,), (1,)), ((), ())), preferred_element_type=jnp.float32
    )


def per_device(
    layer_input, output_grad, query_weight, key_weight, value_weight, out_weight, sink_logit
):
    whole_input, whole_grad = (
        lax.all_gather(layer_input, "tp", axis=1, tiled=True),
        lax.all_gather(output_grad, "tp", axis=1, tiled=True),
    )
    tok_rows = whole_input.shape[0]
    query_cols = query_weight.shape[1]
    key_cols = key_weight.shape[1]
    key_heads = key_cols // HEAD
    group_size = HEADS // KV_HEADS
    scaling = HEAD ** (-0.5)
    queries = jnp.dot(whole_input, query_weight, preferred_element_type=jnp.float32).astype(
        jnp.bfloat16
    )
    key_rows = jnp.dot(whole_input, key_weight, preferred_element_type=jnp.float32).astype(
        jnp.bfloat16
    )
    value_rows = jnp.dot(whole_input, value_weight, preferred_element_type=jnp.float32).astype(
        jnp.bfloat16
    )
    out_rows_grad = contract_cols(whole_grad, out_weight).astype(jnp.bfloat16)
    joined = jnp.concatenate([key_rows, value_rows], axis=1)
    band = extended(joined, (("sp", 0),), WINDOW)
    band_rows = band.shape[0]
    band_keys = band[:, :key_cols].reshape(band_rows, key_heads, HEAD)
    band_values = band[:, key_cols:].reshape(band_rows, key_heads, HEAD)
    shard_index = lax.axis_index("sp")
    seq_total = tok_rows * lax.axis_size("sp")
    query_pos = shard_index * tok_rows + jnp.arange(tok_rows, dtype=jnp.int32)
    key_pos = shard_index * tok_rows - WINDOW + jnp.arange(band_rows, dtype=jnp.int32)
    in_window = (
        (jnp.abs(query_pos[:, None] - key_pos[None, :]) <= WINDOW)
        & (key_pos[None, :] >= 0)
        & (key_pos[None, :] < seq_total)
    )
    query_heads = queries.reshape(tok_rows, key_heads, group_size, HEAD)
    grad_heads = out_rows_grad.reshape(tok_rows, key_heads, group_size, HEAD)
    scores = (
        jnp.einsum("qkgd,skd->kgqs", query_heads, band_keys, preferred_element_type=jnp.float32)
        * scaling
    )
    scores = jnp.where(in_window[None, None], scores, masked_score)
    sink_column = sink_logit.reshape(key_heads, group_size)[:, :, None]
    row_max = jnp.maximum(jnp.max(scores, axis=-1), sink_column)
    row_total = jnp.sum(jnp.exp(scores - row_max[..., None]), axis=-1) + jnp.exp(
        sink_column - row_max
    )
    log_total = row_max + jnp.log(row_total)
    soft_weights = jnp.exp(scores - log_total[..., None])
    soft_rounded = soft_weights.astype(jnp.bfloat16)
    attended = jnp.einsum(
        "kgqs,skd->qkgd", soft_rounded, band_values, preferred_element_type=jnp.float32
    ).astype(jnp.bfloat16)
    row_dots = jnp.sum(
        grad_heads.astype(jnp.float32) * attended.astype(jnp.float32), axis=-1
    ).transpose(1, 2, 0)
    prob_grads = jnp.einsum(
        "qkgd,skd->kgqs", grad_heads, band_values, preferred_element_type=jnp.float32
    )
    score_grads = (soft_weights * (prob_grads - row_dots[..., None])).astype(jnp.bfloat16)
    query_grads = (
        jnp.einsum("kgqs,skd->qkgd", score_grads, band_keys, preferred_element_type=jnp.float32)
        * scaling
    )
    query_grads = query_grads.astype(jnp.bfloat16).reshape(tok_rows, query_cols)
    band_key_grads = (
        jnp.einsum("kgqs,qkgd->skd", score_grads, query_heads, preferred_element_type=jnp.float32)
        * scaling
    )
    band_value_grads = jnp.einsum(
        "kgqs,qkgd->skd", soft_rounded, grad_heads, preferred_element_type=jnp.float32
    )
    band_grads = jnp.concatenate(
        [
            band_key_grads.reshape(band_rows, key_cols),
            band_value_grads.reshape(band_rows, key_cols),
        ],
        axis=1,
    )
    sink_part = -jnp.sum(jnp.exp(sink_column - log_total) * row_dots, axis=-1).reshape(-1)
    sink_grad = lax.psum(sink_part, "sp")
    attended_rows = attended.reshape(tok_rows, query_cols)
    input_cols = whole_input
    early_sums = lax.psum_scatter(
        jnp.concatenate(
            [contract_rows(input_cols, query_grads), contract_rows(whole_grad, attended_rows)],
            axis=1,
        ),
        "sp",
        scatter_dimension=0,
        tiled=True,
    )
    returned_low = passed_along(band_grads[:WINDOW].astype(jnp.bfloat16), "sp", -1).astype(
        jnp.float32
    )
    returned_high = passed_along(
        band_grads[band_rows - WINDOW :].astype(jnp.bfloat16), "sp", 1
    ).astype(jnp.float32)
    own_rows = band_grads[WINDOW : WINDOW + tok_rows]
    own_rows = own_rows.at[tok_rows - WINDOW :].add(returned_low)
    own_rows = own_rows.at[:WINDOW].add(returned_high)
    key_grads = own_rows[:, :key_cols].astype(jnp.bfloat16)
    value_grads = own_rows[:, key_cols:].astype(jnp.bfloat16)
    input_cols = whole_input
    late_sums = lax.psum_scatter(
        jnp.concatenate(
            [contract_rows(input_cols, key_grads), contract_rows(input_cols, value_grads)], axis=1
        ),
        "sp",
        scatter_dimension=0,
        tiled=True,
    )
    query_part = early_sums[:, :query_cols]
    out_part = early_sums[:, query_cols:]
    key_part = late_sums[:, :key_cols]
    value_part = late_sums[:, key_cols:]
    partials = (
        contract_cols(query_grads, query_weight)
        + contract_cols(key_grads, key_weight)
        + contract_cols(value_grads, value_weight)
    )
    input_grad = lax.psum_scatter(
        partials.astype(jnp.bfloat16), "tp", scatter_dimension=1, tiled=True
    )
    return (input_grad, query_part, key_part, value_part, out_part.T, sink_grad)


def solution(mesh):
    placed = (
        P("sp", "tp"),
        P("sp", "tp"),
        P(None, "tp"),
        P(None, "tp"),
        P(None, "tp"),
        P("tp", None),
        P("tp"),
    )
    return jax.shard_map(
        per_device,
        mesh=mesh,
        in_specs=placed,
        out_specs=(
            P("sp", "tp"),
            P("sp", "tp"),
            P("sp", "tp"),
            P("sp", "tp"),
            P("tp", "sp"),
            P("tp"),
        ),
        check_vma=False,
    )
```

profile of v0, /device:TPU:0, one launch (start us, length us, event | category | flops | bytes accessed | tf_op | source)
XLA Modules:
  0.0 551.2 jit_solution(13101381408331590690)
XLA Ops:
  10.3 20.2 %all-gather.3.cloned.1.call-done = bf16[160,4096]{1,0:T(8,128)(2,1)} async-done(((bf16[160,1024]{1,0:T(8,128)(2,1)}), bf16[160,4096]{1,0:T(8,128)(2,1)}) %all-gather.3.cloned.1.call-update) | async-done | bytes 1310736 | tf_op jit(solution)/shard_map/all_gather | solution.py:54
  30.5 2.0 convolution_convert_fusion.3
  32.5 2.1 convolution_convert_fusion.4
  36.0 4.0 collective-permute-start
  41.3 1.5 convolution_convert_fusion.2
  42.8 7.4 %all-gather.5.cloned.1.call-done = bf16[160,4096]{1,0:T(8,128)(2,1)} async-done(((bf16[160,1024]{1,0:T(8,128)(2,1)}), bf16[160,4096]{1,0:T(8,128)(2,1)}) %all-gather.5.cloned.1.call-update) | async-done | bytes 1310736 | tf_op jit(solution)/shard_map/all_gather | solution.py:55
  50.2 4.8 convolution_convert_fusion.1
  55.0 1.6 reshape.179
  56.7 1.6 reshape.177
  60.1 1.7 reshape.178
  61.8 1.7 reshape.176
  63.5 1.6 fusion.39
  68.7 1.3 collective-permute-start.2
  70.0 4.6 collective-permute-start.3
  74.6 1.6 collective-permute-done.2
  76.3 2.6 collective-permute-done.3
  80.5 3.8 pad_maximum_fusion.1
  84.3 1.7 copy.37
  86.1 1.6 reshape.183
  87.7 1.5 fusion.12
  90.1 1.6 reshape.180
  91.7 2.4 convolution_bitcast_fusion.1
  94.1 1.3 convolution_bitcast_fusion
  95.4 6.4 %pad_maximum_fusion = f32[4096,1024]{0,1:T(8,128)} fusion(f32[4096,512]{0,1:T(8,128)S(1)} %convolution_bitcast_fusion, f32[4096,512]{0,1:T(8,128)S(1)} %convolution_bitcast_fusion.1), kind=kLoop, calls=%fused_computation | loop fusion | flops 4194304 | bytes 33554432 | tf_op jit(solution)/shard_map/concatenate | solution.py:136
  105.2 1.4 copy-done.3
  106.6 2.6 fusion.1
  109.4 22.6 %psum.7 = f32[4]{0:T(128)} all-reduce(f32[4]{0:T(128)S(1)} %neg.7), channel_id=1, replica_groups=mesh['sp'=8,'tp'=4] {'sp'}, use_global_device_ids=true, to_apply=%region_7.8 | all-reduce | flops 4 | bytes 32 | tf_op jit(solution)/shard_map/psum | solution.py:132
  132.0 101.1 %reduce-scatter.8.cloned.1.call-done = f32[512,512]{0,1:T(8,128)} async-done(((f32[4096,512]{0,1:T(8,128)}), f32[512,512]{0,1:T(8,128)}) %reduce-scatter.8.cloned.1.call-update) | async-done | bytes 1048592 | tf_op jit(solution)/shard_map/reduce_scatter | solution.py:156
  236.3 279.8 %reduce-scatter.6.cloned.1.call-done = f32[512,1024]{0,1:T(8,128)} async-done(((f32[4096,1024]{0,1:T(8,128)}), f32[512,1024]{0,1:T(8,128)}) %reduce-scatter.6.cloned.1.call-update) | async-done | bytes 2097168 | tf_op jit(solution)/shard_map/reduce_scatter | solution.py:135
  516.1 2.7 slice_bitcast_fusion
  518.8 1.3 copy.38
  520.1 24.6 %reduce-scatter.4.cloned.1.call-done = bf16[160,1024]{1,0:T(8,128)(2,1)} async-done(((bf16[160,4096]{1,0:T(8,128)(2,1)}), bf16[160,1024]{1,0:T(8,128)(2,1)}) %reduce-scatter.4.cloned.1.call-update) | async-done | bytes 327696 | tf_op jit(solution)/shard_map/reduce_scatter | solution.py:173
  (76 shorter events, 20.4 us)
Async XLA Ops:
  7.2 23.3 %copy-start = (bf16[4096,256]{1,0:T(8,128)(2,1)S(1)}, bf16[4096,256]{1,0:T(8,128)(2,1)}, u32[]{:S(2)}) copy-start(bf16[4096,256]{1,0:T(8,128)(2,1)} %param.15) | copy-start | bytes 6291460
  7.2 23.3 %all-gather.3.cloned.1.call-start = ((), (), s32[]{:S(2)}) async-start(), calls=%async_computation.3 | async-start | bytes 1638400 | tf_op jit(solution)/shard_map/all_gather | solution.py:54
  7.9 42.3 %all-gather.5.cloned.1.call-start = ((), (), s32[]{:S(2)}) async-start(), calls=%async_computation.4 | async-start | bytes 1638400 | tf_op jit(solution)/shard_map/all_gather | solution.py:55
  8.7 224.4 %reduce-scatter.8.cloned.1.call-start = ((), (), s32[]{:S(2)}) async-start(), calls=%async_computation.7 | async-start | bytes 9437184 | tf_op jit(solution)/shard_map/reduce_scatter | solution.py:156
  30.5 2.0 copy-start.1
  30.5 10.8 %copy-start.2 = (bf16[4096,512]{1,0:T(8,128)(2,1)S(1)}, bf16[4096,512]{1,0:T(8,128)(2,1)}, u32[]{:S(2)}) copy-start(bf16[4096,512]{1,0:T(8,128)(2,1)} %param.13) | copy-start | bytes 12582916
  34.6 0.6 copy-start.12
  36.0 22.3 %collective-permute-start = (bf16[128,512]{1,0:T(8,128)(2,1)}, bf16[128,512]{1,0:T(8,128)(2,1)}, u32[]{:S(2)}, u32[]{:S(2)}) collective-permute-start(bf16[128,512]{1,0:T(8,128)(2,1)} %get-tuple-element.50), channel_id=1, source_target_pairs={{0,4},{4,8},{8,12},{12,16},{16,20},{20,24},{24,28},{1,5},{5,9},{9,... | collective-permute-start | bytes 393224 | tf_op jit(solution)/shard_map/ppermute | solution.py:23
  40.0 18.3 %collective-permute-start.1 = (bf16[128,512]{1,0:T(8,128)(2,1)}, bf16[128,512]{1,0:T(8,128)(2,1)}, u32[]{:S(2)}, u32[]{:S(2)}) collective-permute-start(bf16[128,512]{1,0:T(8,128)(2,1)} %get-tuple-element.51), channel_id=1, source_target_pairs={{4,0},{8,4},{12,8},{16,12},{20,16},{24,20},{28,24},{5,1},{9,5},{13... | collective-permute-start | bytes 393224 | tf_op jit(solution)/shard_map/ppermute | solution.py:25
  63.5 2.3 copy-start.7
  63.5 2.9 copy-start.8
  66.4 1.5 copy-start.13
  67.8 0.8 copy-start.5
  68.7 7.5 %collective-permute-start.2 = (bf16[128,512]{1,0:T(8,128)(2,1)S(1)}, bf16[128,512]{1,0:T(8,128)(2,1)S(1)}, u32[]{:S(2)}, u32[]{:S(2)}) collective-permute-start(bf16[128,512]{1,0:T(8,128)(2,1)S(1)} %get-tuple-element.47), channel_id=1, source_target_pairs={{4,0},{8,4},{12,8},{16,12},{20,16},{24,20},{28,24},{5,1},{9,5},{13... | collective-permute-start | bytes 393224 | tf_op jit(solution)/shard_map/ppermute | solution.py:35
  70.0 8.9 %collective-permute-start.3 = (bf16[128,512]{1,0:T(8,128)(2,1)S(1)}, bf16[128,512]{1,0:T(8,128)(2,1)S(1)}, u32[]{:S(2)}, u32[]{:S(2)}) collective-permute-start(bf16[128,512]{1,0:T(8,128)(2,1)S(1)} %get-tuple-element.46), channel_id=1, source_target_pairs={{0,4},{4,8},{8,12},{12,16},{16,20},{20,24},{24,28},{1,5},{5,9},{9,... | collective-permute-start | bytes 393224 | tf_op jit(solution)/shard_map/ppermute | solution.py:35
  79.0 0.7 copy-start.10
  84.3 431.8 %reduce-scatter.6.cloned.1.call-start = ((), (), s32[]{:S(2)}) async-start(), calls=%async_computation.6 | async-start | bytes 18874368 | tf_op jit(solution)/shard_map/reduce_scatter | solution.py:135
  91.7 2.4 copy-start.6
  91.7 2.4 copy-start.14
  101.8 0.9 copy-start.11
  101.8 442.9 %reduce-scatter.4.cloned.1.call-start = ((), (), s32[]{:S(2)}) async-start(), calls=%async_computation.5 | async-start | bytes 1638400 | tf_op jit(solution)/shard_map/reduce_scatter | solution.py:173
  102.7 1.6 copy-start.4
  104.3 2.2 copy-start.3
  104.3 2.2 copy-start.9
Sparse Core Ops, SparseCore 0:
  9.6 20.8 all-gather.2
  32.0 18.1 all-gather.4
  84.4 148.6 reduce-scatter.7
  236.7 279.3 reduce-scatter.5
  519.1 25.5 reduce-scatter.3
where the time goes:
time: 552 us; the launch traced here: 551 us
  waiting for transfers between devices  439 us (80%)
  matrix products  25.6 us (5%)
  local copies, waits for them, and re-layouts  25.1 us (5%)
  blocking collectives  22.6 us (4%)
  between operations  14.1 us (3%)
  other arithmetic  13.7 us (2%)
  starting transfers between devices  11.5 us (2%)
    reduce_scatter x1, waiting for transfers between devices, per_device(): lax.psum_scatter(jnp.concatenate([contract_rows(input_cols, query_grads),...  280 us
    reduce_scatter x1, waiting for transfers between devices, per_device(): lax.psum_scatter(jnp.concatenate([contract_rows(input_cols, key_grads), c...  101 us
    reduce_scatter x1, waiting for transfers between devices, per_device(): lax.psum_scatter(partials.astype(jnp.bfloat16), 'tp', scatter_dimension=1...  24.6 us
    psum x1, blocking collectives, per_device(): sink_grad = lax.psum(sink_part, 'sp')  22.6 us
    all_gather x1, waiting for transfers between devices, per_device(): lax.all_gather(layer_input, 'tp', axis=1, tiled=True)  20.2 us
  transfers between devices with their start and end apart: 9, of which 7 were waited for; matrix products, arithmetic and copies ran while one was open for 8% of the time, Pallas kernels for 0%

commit v1 on v0

--- a/solution.py
+++ b/solution.py
@@ -131,16 +131,13 @@
     sink_part = -jnp.sum(jnp.exp(sink_column - log_total) * row_dots, axis=-1).reshape(-1)
     sink_grad = lax.psum(sink_part, "sp")
     attended_rows = attended.reshape(tok_rows, query_cols)
-    input_cols = whole_input
-    early_sums = lax.psum_scatter(
-        jnp.concatenate(
-            [contract_rows(input_cols, query_grads), contract_rows(whole_grad, attended_rows)],
-            axis=1,
-        ),
-        "sp",
-        scatter_dimension=0,
-        tiled=True,
+    input_block = lax.all_to_all(whole_input, "sp", 1, 0, tiled=True)
+    grad_block = lax.all_to_all(whole_grad, "sp", 1, 0, tiled=True)
+    early_rows = lax.all_gather(
+        jnp.concatenate([query_grads, attended_rows], axis=1), "sp", axis=0, tiled=True
     )
+    query_part = contract_rows(input_block, early_rows[:, :query_cols])
+    out_part = contract_rows(early_rows[:, query_cols:], grad_block)
     returned_low = passed_along(band_grads[:WINDOW].astype(jnp.bfloat16), "sp", -1).astype(
         jnp.float32
     )
@@ -152,19 +149,11 @@
     own_rows = own_rows.at[:WINDOW].add(returned_high)
     key_grads = own_rows[:, :key_cols].astype(jnp.bfloat16)
     value_grads = own_rows[:, key_cols:].astype(jnp.bfloat16)
-    input_cols = whole_input
-    late_sums = lax.psum_scatter(
-        jnp.concatenate(
-            [contract_rows(input_cols, key_grads), contract_rows(input_cols, value_grads)], axis=1
-        ),
-        "sp",
-        scatter_dimension=0,
-        tiled=True,
+    late_rows = lax.all_gather(
+        jnp.concatenate([key_grads, value_grads], axis=1), "sp", axis=0, tiled=True
     )
-    query_part = early_sums[:, :query_cols]
-    out_part = early_sums[:, query_cols:]
-    key_part = late_sums[:, :key_cols]
-    value_part = late_sums[:, key_cols:]
+    key_part = contract_rows(input_block, late_rows[:, :key_cols])
+    value_part = contract_rows(input_block, late_rows[:, key_cols:])
     partials = (
         contract_cols(query_grads, query_weight)
         + contract_cols(key_grads, key_weight)
@@ -173,7 +162,7 @@
     input_grad = lax.psum_scatter(
         partials.astype(jnp.bfloat16), "tp", scatter_dimension=1, tiled=True
     )
-    return (input_grad, query_part, key_part, value_part, out_part.T, sink_grad)
+    return (input_grad, query_part, key_part, value_part, out_part, sink_grad)
 
 
 def solution(mesh):

time: 552 us -> 248 us (0.45)
  waiting for transfers between devices: 439 us -> 94.8 us
  blocking collectives: 22.6 us -> 47.5 us
  starting transfers between devices: 11.5 us -> 21.1 us
  matrix products: 25.6 us -> 34.4 us
  other arithmetic: 13.7 us -> 5.94 us
    reduce_scatter x2 -> x0, waiting for transfers between devices: 381 us -> none  [the longest x1 280 us: per_device(): lax.psum_scatter(jnp.concatenate([contract_rows(input_cols, query_grads),...]
    all_to_all x0 -> x2, waiting for transfers between devices: none -> 33.8 us  [the longest x1 33.8 us: per_device(): input_block = lax.all_to_all(whole_input, 'sp', 1, 0, tiled=True)]
    psum x1, blocking collectives: 22.6 us -> 47.5 us  [per_device(): sink_grad = lax.psum(sink_part, 'sp')]
    all_to_all x0 -> x2, starting transfers between devices: none -> 9.79 us  [the longest x1 6.07 us: per_device(): input_block = lax.all_to_all(whole_input, 'sp', 1, 0, tiled=True)]
    all_gather x0 -> x2, waiting for transfers between devices: none -> 9.16 us  [the longest x1 9.16 us: per_device(): lax.all_gather(jnp.concatenate([query_grads, attended_rows], axis=1), 'sp...]
    concatenate x2 -> x1, other arithmetic: 10.1 us -> 1.76 us  [per_device(): jnp.concatenate([query_grads, attended_rows], axis=1)]
    dot_general x4, matrix products: 5.16 us -> 12.5 us  [contract_rows(): lax.dot_general(left, right, (((0,), (0,)), ((), ())), preferred_element_...]
    reduce_scatter x1, waiting for transfers between devices: 24.6 us -> 18.6 us  [per_device(): lax.psum_scatter(partials.astype(jnp.bfloat16), 'tp', scatter_dimension=1...]
  transfers between devices with their start and end apart: 9 -> 11, of which waited for: 7 -> 7; matrix products, arithmetic and copies ran while one was open for 8% -> 21% of each run, Pallas kernels for 0% -> 0%
where the time goes in v1:
time: 248 us; the launch traced here: 247 us
  waiting for transfers between devices  94.8 us (38%)
  blocking collectives  47.5 us (19%)
  matrix products  34.4 us (14%)
  local copies, waits for them, and re-layouts  29.1 us (12%)
  starting transfers between devices  21.1 us (9%)
  between operations  14 us (6%)
  other arithmetic  5.94 us (2%)
    psum x1, blocking collectives, per_device(): sink_grad = lax.psum(sink_part, 'sp')  47.5 us
    all_to_all x1, waiting for transfers between devices, per_device(): input_block = lax.all_to_all(whole_input, 'sp', 1, 0, tiled=True)  33.8 us
    all_gather x1, waiting for transfers between devices, per_device(): lax.all_gather(layer_input, 'tp', axis=1, tiled=True)  20.2 us
    reduce_scatter x1, waiting for transfers between devices, per_device(): lax.psum_scatter(partials.astype(jnp.bfloat16), 'tp', scatter_dimension=1...  18.6 us
    unnamed x34, local copies, waits for them, and re-layouts  12.5 us
    dot_general x4, matrix products, contract_rows(): lax.dot_general(left, right, (((0,), (0,)), ((), ())), preferred_element_...  12.5 us
    all_gather x1, waiting for transfers between devices, per_device(): lax.all_gather(jnp.concatenate([query_grads, attended_rows], axis=1), 'sp...  9.16 us
    dot_general x4, matrix products, contract_cols(): lax.dot_general(left, right, (((1,), (1,)), ((), ())), preferred_element_...  9.07 us
  transfers between devices with their start and end apart: 11, of which 7 were waited for; matrix products, arithmetic and copies ran while one was open for 21% of the time, Pallas kernels for 0%

profile of v1, /device:TPU:0, one launch (start us, length us, event | category | flops | bytes accessed | tf_op | source)
XLA Modules:
  0.0 246.9 jit_solution(17881968842394608186)
XLA Ops:
  10.3 20.2 %all-gather.5.cloned.1.call-done = bf16[160,4096]{1,0:T(8,128)(2,1)} async-done(((bf16[160,1024]{1,0:T(8,128)(2,1)}), bf16[160,4096]{1,0:T(8,128)(2,1)}) %all-gather.5.cloned.1.call-update) | async-done | bytes 1310736 | tf_op jit(solution)/shard_map/all_gather | solution.py:54
  30.5 2.0 convolution_convert_fusion.3
  32.5 2.1 convolution_convert_fusion.4
  36.0 4.0 %collective-permute-start = (bf16[128,512]{1,0:T(8,128)(2,1)}, bf16[128,512]{1,0:T(8,128)(2,1)}, u32[]{:S(2)}, u32[]{:S(2)}) collective-permute-start(bf16[128,512]{1,0:T(8,128)(2,1)} %get-tuple-element.58), channel_id=1, source_target_pairs={{0,4},{4,8},{8,12},{12,16},{16,20},{20,24},{24,28},{1,5},{5,9},{9,... | collective-permute-start | bytes 393224 | tf_op jit(solution)/shard_map/ppermute | solution.py:23
  42.8 7.4 %all-gather.7.cloned.1.call-done = bf16[160,4096]{1,0:T(8,128)(2,1)} async-done(((bf16[160,1024]{1,0:T(8,128)(2,1)}), bf16[160,4096]{1,0:T(8,128)(2,1)}) %all-gather.7.cloned.1.call-update) | async-done | bytes 1310736 | tf_op jit(solution)/shard_map/all_gather | solution.py:55
  50.2 4.8 %convolution_convert_fusion.1 = bf16[160,512]{1,0:T(8,128)(2,1)} fusion(bf16[160,4096]{1,0:T(8,128)(2,1)} %all-gather.7.cloned.1.call-done, bf16[512,4096]{1,0:T(8,128)(2,1)} %param.16), kind=kOutput, calls=%fused_computation.27 | convolution fusion | flops 671170560 | bytes 5668864 | tf_op jit(solution)/shard_map/dot_general | solution.py:45
  55.0 1.6 reshape.183
  56.7 1.6 reshape.185
  60.1 1.7 reshape.182
  65.0 1.7 reshape.184
  66.7 2.2 convolution_bitcast_fusion.4
  73.1 4.6 %collective-permute-start.3 = (bf16[128,512]{1,0:T(8,128)(2,1)S(1)}, bf16[128,512]{1,0:T(8,128)(2,1)S(1)}, u32[]{:S(2)}, u32[]{:S(2)}) collective-permute-start(bf16[128,512]{1,0:T(8,128)(2,1)S(1)} %get-tuple-element.54), channel_id=1, source_target_pairs={{0,4},{4,8},{8,12},{12,16},{16,20},{20,24},{24,28},{1,5},{5,9},{9,... | collective-permute-start | bytes 393224 | tf_op jit(solution)/shard_map/ppermute | solution.py:35
  77.7 1.6 collective-permute-done.2
  79.3 2.6 %collective-permute-done.3 = bf16[128,512]{1,0:T(8,128)(2,1)S(1)} collective-permute-done((bf16[128,512]{1,0:T(8,128)(2,1)S(1)}, bf16[128,512]{1,0:T(8,128)(2,1)S(1)}, u32[]{:S(2)}, u32[]{:S(2)}) %collective-permute-start.3) | collective-permute-done | bytes 131104 | tf_op jit(solution)/shard_map/ppermute | solution.py:35
  85.2 1.6 reshape.186
  86.8 1.7 copy.71
  88.5 1.6 reshape.189
  90.2 1.8 pad_maximum_fusion.1
  93.2 6.1 %all-to-all-start = ((bf16[160,8,512]{2,0,1:T(8,128)(2,1)}), bf16[160,8,512]{2,0,1:T(8,128)(2,1)}, u32[]{:S(2)}, u32[]{:S(2)}) async-start(bf16[160,8,512]{2,0,1:T(8,128)(2,1)} %bitcast.81), calls=%async_computation.1 | async-start | bytes 2621440 | tf_op jit(solution)/shard_map/all_to_all | solution.py:134
  103.2 2.6 %fusion.1 = bf16[160,4096]{1,0:T(8,128)(2,1)} fusion(f32[160,4096]{1,0:T(8,128)S(1)} %fusion.33, f32[160,4096]{1,0:T(8,128)S(1)} %fusion.35, bf16[160,512]{1,0:T(8,128)(2,1)S(1)} %copy-done.11, bf16[4096,512]{1,0:T(8,128)(2,1)S(1)} %copy-done.5), kind=kOutput, calls=%fused_computation.2 | convolution fusion | flops 673054720 | bytes 10911744 | tf_op jit(solution)/shard_map/dot_general | solution.py:45
  108.3 33.8 %all-to-all-done = bf16[160,8,512]{2,0,1:T(8,128)(2,1)} async-done(((bf16[160,8,512]{2,0,1:T(8,128)(2,1)}), bf16[160,8,512]{2,0,1:T(8,128)(2,1)}, u32[]{:S(2)}, u32[]{:S(2)}) %all-to-all-start) | async-done | bytes 1310752 | tf_op jit(solution)/shard_map/all_to_all | solution.py:134
  142.0 3.7 %all-to-all-start.1 = ((bf16[160,8,512]{2,0,1:T(8,128)(2,1)}), bf16[160,8,512]{2,0,1:T(8,128)(2,1)S(1)}, u32[]{:S(2)}, u32[]{:S(2)}) async-start(bf16[160,8,512]{2,0,1:T(8,128)(2,1)} %bitcast.78), calls=%async_computation.2 | async-start | bytes 2621440 | tf_op jit(solution)/shard_map/all_to_all | solution.py:135
  146.0 47.5 %psum.7 = f32[4]{0:T(128)} all-reduce(f32[4]{0:T(128)S(1)} %neg.7), channel_id=1, replica_groups=mesh['sp'=8,'tp'=4] {'sp'}, use_global_device_ids=true, to_apply=%region_5.6 | all-reduce | flops 4 | bytes 32 | tf_op jit(solution)/shard_map/psum | solution.py:132
  193.5 2.8 %convolution_bitcast_fusion.3 = f32[512,256]{0,1:T(8,128)} fusion(bf16[1280,512]{1,0:T(8,128)(2,1)} %bitcast.16, bf16[1280,512]{1,0:T(8,128)(2,1)} %all-gather.11.cloned.1.call-done), kind=kOutput, calls=%fused_computation.19 | convolution fusion | flops 335544320 | bytes 2490368 | tf_op jit(solution)/shard_map/dot_general | solution.py:39
  196.4 2.0 copy.75
  198.4 2.8 %convolution_bitcast_fusion.2 = f32[512,256]{0,1:T(8,128)} fusion(bf16[1280,512]{1,0:T(8,128)(2,1)} %bitcast.16, bf16[1280,512]{1,0:T(8,128)(2,1)} %all-gather.11.cloned.1.call-done), kind=kOutput, calls=%fused_computation.18 | convolution fusion | flops 335544320 | bytes 2490368 | tf_op jit(solution)/shard_map/dot_general | solution.py:39
  201.2 2.0 copy.76
  203.3 9.2 %all-gather.9.cloned.1.call-done = bf16[1280,1024]{1,0:T(8,128)(2,1)} async-done(((bf16[160,1024]{1,0:T(8,128)(2,1)}), bf16[1280,1024]{1,0:T(8,128)(2,1)}) %all-gather.9.cloned.1.call-update) | async-done | bytes 2621456 | tf_op jit(solution)/shard_map/all_gather | solution.py:136
  212.4 3.5 %convolution_bitcast_fusion.1 = f32[512,512]{0,1:T(8,128)} fusion(bf16[1280,512]{1,0:T(8,128)(2,1)} %bitcast.16, bf16[1280,1024]{1,0:T(8,128)(2,1)} %all-gather.9.cloned.1.call-done), kind=kOutput, calls=%fused_computation.9 | convolution fusion | flops 671088640 | bytes 3670016 | tf_op jit(solution)/shard_map/dot_general | solution.py:39
  216.0 2.5 %copy.74 = f32[512,512]{1,0:T(8,128)} copy(f32[512,512]{0,1:T(8,128)} %convolution_bitcast_fusion.1) | data formatting | bytes 2097152
  218.5 3.3 %fusion.7 = f32[512,512]{1,0:T(8,128)} fusion(bf16[1280,512]{1,0:T(8,128)(2,1)S(1)} %bitcast.85, bf16[1280,1024]{1,0:T(8,128)(2,1)} %all-gather.9.cloned.1.call-done), kind=kOutput, calls=%fused_computation.13 | convolution fusion | flops 671088640 | bytes 3670016 | tf_op jit(solution)/shard_map/dot_general | solution.py:39
  221.8 18.6 %reduce-scatter.2.cloned.1.call-done = bf16[160,1024]{1,0:T(8,128)(2,1)} async-done(((bf16[160,4096]{1,0:T(8,128)(2,1)}), bf16[160,1024]{1,0:T(8,128)(2,1)}) %reduce-scatter.2.cloned.1.call-update) | async-done | bytes 327696 | tf_op jit(solution)/shard_map/reduce_scatter | solution.py:162
  (79 shorter events, 27.5 us)
Async XLA Ops:
  7.2 23.3 %copy-start = (bf16[4096,256]{1,0:T(8,128)(2,1)S(1)}, bf16[4096,256]{1,0:T(8,128)(2,1)}, u32[]{:S(2)}) copy-start(bf16[4096,256]{1,0:T(8,128)(2,1)} %param.15) | copy-start | bytes 6291460
  7.2 23.3 %all-gather.5.cloned.1.call-start = ((), (), s32[]{:S(2)}) async-start(), calls=%async_computation.3 | async-start | bytes 1638400 | tf_op jit(solution)/shard_map/all_gather | solution.py:54
  7.9 42.3 %all-gather.7.cloned.1.call-start = ((), (), s32[]{:S(2)}) async-start(), calls=%async_computation.4 | async-start | bytes 1638400 | tf_op jit(solution)/shard_map/all_gather | solution.py:55
  8.7 184.9 %all-gather.11.cloned.1.call-start = ((), (), s32[]{:S(2)}) async-start(), calls=%async_computation.7 | async-start | bytes 1474560 | tf_op jit(solution)/shard_map/all_gather | solution.py:152
  30.5 2.0 copy-start.1
  30.5 10.8 %copy-start.4 = (bf16[4096,512]{1,0:T(8,128)(2,1)S(1)}, bf16[4096,512]{1,0:T(8,128)(2,1)}, u32[]{:S(2)}) copy-start(bf16[4096,512]{1,0:T(8,128)(2,1)} %param.13) | copy-start | bytes 12582916
  34.6 0.6 copy-start.13
  36.0 22.3 %collective-permute-start = (bf16[128,512]{1,0:T(8,128)(2,1)}, bf16[128,512]{1,0:T(8,128)(2,1)}, u32[]{:S(2)}, u32[]{:S(2)}) collective-permute-start(bf16[128,512]{1,0:T(8,128)(2,1)} %get-tuple-element.58), channel_id=1, source_target_pairs={{0,4},{4,8},{8,12},{12,16},{16,20},{20,24},{24,28},{1,5},{5,9},{9,... | collective-permute-start | bytes 393224 | tf_op jit(solution)/shard_map/ppermute | solution.py:23
  40.0 18.3 %collective-permute-start.1 = (bf16[128,512]{1,0:T(8,128)(2,1)}, bf16[128,512]{1,0:T(8,128)(2,1)}, u32[]{:S(2)}, u32[]{:S(2)}) collective-permute-start(bf16[128,512]{1,0:T(8,128)(2,1)} %get-tuple-element.59), channel_id=1, source_target_pairs={{4,0},{8,4},{12,8},{16,12},{20,16},{24,20},{28,24},{5,1},{9,5},{13... | collective-permute-start | bytes 393224 | tf_op jit(solution)/shard_map/ppermute | solution.py:25
  63.4 1.1 copy-start.2
  66.7 2.2 copy-start.3
  66.7 2.2 copy-start.9
  66.7 2.2 copy-start.10
  69.9 0.9 copy-start.14
  70.9 0.8 copy-start.7
  71.8 7.5 %collective-permute-start.2 = (bf16[128,512]{1,0:T(8,128)(2,1)S(1)}, bf16[128,512]{1,0:T(8,128)(2,1)S(1)}, u32[]{:S(2)}, u32[]{:S(2)}) collective-permute-start(bf16[128,512]{1,0:T(8,128)(2,1)S(1)} %get-tuple-element.55), channel_id=1, source_target_pairs={{4,0},{8,4},{12,8},{16,12},{20,16},{24,20},{28,24},{5,1},{9,5},{13... | collective-permute-start | bytes 393224 | tf_op jit(solution)/shard_map/ppermute | solution.py:35
  73.1 8.9 %collective-permute-start.3 = (bf16[128,512]{1,0:T(8,128)(2,1)S(1)}, bf16[128,512]{1,0:T(8,128)(2,1)S(1)}, u32[]{:S(2)}, u32[]{:S(2)}) collective-permute-start(bf16[128,512]{1,0:T(8,128)(2,1)S(1)} %get-tuple-element.54), channel_id=1, source_target_pairs={{0,4},{4,8},{8,12},{12,16},{16,20},{20,24},{24,28},{1,5},{5,9},{9,... | collective-permute-start | bytes 393224 | tf_op jit(solution)/shard_map/ppermute | solution.py:35
  82.8 129.7 %all-gather.9.cloned.1.call-start = ((), (), s32[]{:S(2)}) async-start(), calls=%async_computation.6 | async-start | bytes 2949120 | tf_op jit(solution)/shard_map/all_gather | solution.py:136
  93.2 6.1 %copy-start.12 = (bf16[160,512]{1,0:T(8,128)(2,1)S(1)}, bf16[160,512]{1,0:T(8,128)(2,1)}, u32[]{:S(2)}) copy-start(bf16[160,512]{1,0:T(8,128)(2,1)} %convert.9) | copy-start | bytes 491524
  93.2 48.8 %all-to-all-start = ((bf16[160,8,512]{2,0,1:T(8,128)(2,1)}), bf16[160,8,512]{2,0,1:T(8,128)(2,1)}, u32[]{:S(2)}, u32[]{:S(2)}) async-start(bf16[160,8,512]{2,0,1:T(8,128)(2,1)} %bitcast.81), calls=%async_computation.1 | async-start | bytes 2621440 | tf_op jit(solution)/shard_map/all_to_all | solution.py:134
  99.3 141.1 %reduce-scatter.2.cloned.1.call-start = ((), (), s32[]{:S(2)}) async-start(), calls=%async_computation.5 | async-start | bytes 1638400 | tf_op jit(solution)/shard_map/reduce_scatter | solution.py:162
  99.4 1.6 copy-start.6
  101.0 2.2 copy-start.5
  101.0 2.2 copy-start.11
  105.8 1.3 copy-start.8
  142.0 76.5 %all-to-all-start.1 = ((bf16[160,8,512]{2,0,1:T(8,128)(2,1)}), bf16[160,8,512]{2,0,1:T(8,128)(2,1)S(1)}, u32[]{:S(2)}, u32[]{:S(2)}) async-start(bf16[160,8,512]{2,0,1:T(8,128)(2,1)} %bitcast.78), calls=%async_computation.2 | async-start | bytes 2621440 | tf_op jit(solution)/shard_map/all_to_all | solution.py:135
Sparse Core Ops, SparseCore 0:
  9.6 20.8 all-gather.4
  32.0 18.1 all-gather.6
  82.9 58.5 all-gather.10
  144.1 68.2 all-gather.8
  215.4 24.9 reduce-scatter.1

commit v2 on v1

--- a/solution.py
+++ b/solution.py
@@ -1,6 +1,10 @@
+import functools
+
 import jax
 import jax.numpy as jnp
 from jax import lax
+from jax.experimental import pallas as pl
+from jax.experimental.pallas import tpu as pltpu
 from jax.sharding import PartitionSpec as P
 
 HEADS = 16
@@ -165,6 +169,491 @@
     return (input_grad, query_part, key_part, value_part, out_part, sink_grad)
 
 
+LANES = 128
+MESH = pl.DeviceIdType.MESH
+VMEM_BYTES = 60 * 1024 * 1024
+
+
+def dot_nn(a, b):
+    return jnp.dot(a, b, preferred_element_type=jnp.float32)
+
+
+def layer_kernel(
+    x_ref, g_ref, wq_hbm, wk_hbm, wv_hbm, wo_hbm, sink_ref,
+    ig_ref, gq_ref, gk_ref, gv_ref, go_ref, sg_ref,
+    wq, wk, wv, wo, xg, acc, qs, dos, band, bg, ret_out, ret_in,
+    blk, acts_e, acts_l, part, rs_in, sinks,
+    w_sem, own_sem, ag_send, ag_recv, halo_send, halo_recv, ret_send, ret_recv,
+    a2a_send, a2a_recv, blk_send, blk_recv, up_sem, down_sem, cross_sem, acts_recv,
+    rs_send, rs_recv, sink_send, sink_recv,
+):
+    bf16 = jnp.bfloat16
+    count, tps = lax.axis_size("sp"), lax.axis_size("tp")
+    depth = count // 2
+    s, t = lax.axis_index("sp"), lax.axis_index("tp")
+    z, x = s // 2, s % 2
+    y, core = t // 2, t % 2
+    partner = y * 2 + (1 - core)
+    across = (1 - y) * 2 + core
+    diag = (1 - y) * 2 + (1 - core)
+    rows, feats = x_ref.shape
+    q_cols, k_cols = wq.shape[1], wk.shape[1]
+    block_cols = gq_ref.shape[0]
+    per_slot = feats // block_cols
+    key_heads = k_cols // HEAD
+    group = q_cols // k_cols
+    scaling = HEAD**-0.5
+
+    def remote(src, dst, send, recv, dev_s, dev_t):
+        return pltpu.make_async_remote_copy(
+            src_ref=src, dst_ref=dst, send_sem=send, recv_sem=recv,
+            device_id=(dev_s, dev_t), device_id_type=MESH,
+        )
+
+    weights = [
+        pltpu.make_async_copy(src, dst, w_sem.at[i])
+        for i, (src, dst) in enumerate(((wq_hbm, wq), (wk_hbm, wk), (wv_hbm, wv), (wo_hbm, wo)))
+    ]
+    for copy in weights:
+        copy.start()
+    own = [
+        pltpu.make_async_copy(ref, xg.at[t, a], own_sem.at[a])
+        for a, ref in enumerate((x_ref, g_ref))
+    ]
+    for copy in own:
+        copy.start()
+
+    barrier = pltpu.get_barrier_semaphore()
+    for peer in (partner, across, diag):
+        pl.semaphore_signal(barrier, inc=1, device_id=(s, peer), device_id_type=MESH)
+    for d in range(1, count):
+        pl.semaphore_signal(
+            barrier, inc=1, device_id=((s + d) % count, t), device_id_type=MESH
+        )
+    pl.semaphore_wait(barrier, 3 + count - 1)
+
+    sources = (x_ref, g_ref)
+    to_across = [
+        remote(sources[a], xg.at[t, a], ag_send.at[0, a], ag_recv.at[0, a], s, across)
+        for a in range(2)
+    ]
+    to_partner = [
+        remote(sources[a], xg.at[t, a], ag_send.at[1, a], ag_recv.at[1, a], s, partner)
+        for a in range(2)
+    ]
+    relay = [
+        remote(xg.at[across, a], xg.at[across, a], ag_send.at[2, a], ag_recv.at[2, a], s, partner)
+        for a in range(2)
+    ]
+    for copy in to_across + to_partner:
+        copy.start()
+
+    def project_input(slot, first):
+        cells = xg[slot, 0]
+        span = pl.ds(pl.multiple_of(slot * feats, feats), feats)
+        at = 0
+        for w in (wq, wk, wv):
+            cols = w.shape[1]
+            term = dot_nn(cells, w[span, :])
+            acc[:, at : at + cols] = term if first else acc[:, at : at + cols] + term
+            at += cols
+
+    def project_grad(slot, first):
+        span = pl.ds(pl.multiple_of(slot * feats, feats), feats)
+        term = contract_cols(xg[slot, 1], wo[:, span])
+        lo = q_cols + 2 * k_cols
+        acc[:, lo:] = term if first else acc[:, lo:] + term
+
+    for copy in own + weights:
+        copy.wait()
+    project_input(t, True)
+    project_grad(t, True)
+    to_partner[0].wait_recv()
+    project_input(partner, False)
+    to_partner[1].wait_recv()
+    project_grad(partner, False)
+    to_across[0].wait_recv()
+    relay[0].start()
+    project_input(across, False)
+    relay[0].wait_recv()
+    project_input(diag, False)
+
+    mid = pl.ds(WINDOW, rows)
+    band[mid, :] = acc[:, q_cols : q_cols + 2 * k_cols].astype(bf16)
+    qs[...] = acc[:, :q_cols].astype(bf16)
+    has_prev, has_next = s > 0, s < count - 1
+    prev, nxt = lax.rem(s + count - 1, count), lax.rem(s + 1, count)
+    low, high = pl.ds(0, WINDOW), pl.ds(WINDOW + rows, WINDOW)
+    tail_copy = remote(
+        band.at[pl.ds(rows, WINDOW)], band.at[low], halo_send.at[0], halo_recv.at[0], nxt, t
+    )
+    head_copy = remote(
+        band.at[pl.ds(WINDOW, WINDOW)], band.at[high], halo_send.at[1], halo_recv.at[1], prev, t
+    )
+
+    @pl.when(has_next)
+    def _():
+        tail_copy.start()
+
+    @pl.when(has_prev)
+    def _():
+        head_copy.start()
+
+    to_across[1].wait_recv()
+    relay[1].start()
+    project_grad(across, False)
+    relay[1].wait_recv()
+    project_grad(diag, False)
+    dos[...] = acc[:, q_cols + 2 * k_cols :].astype(bf16)
+
+    def a2a_source(j):
+        lane = (j % per_slot) * block_cols + t * LANES
+        return xg.at[j // per_slot, :, :, pl.ds(pl.multiple_of(lane, LANES), LANES)]
+
+    own_block = pltpu.make_async_copy(a2a_source(s), blk.at[t, s], own_sem.at[2])
+    own_block.start()
+    a2a = []
+    for d in range(1, count):
+        j = (s + d) % count
+        a2a.append(
+            remote(a2a_source(j), blk.at[t, s], a2a_send.at[d], a2a_recv.at[d], j, t)
+        )
+        a2a[-1].start()
+
+    @pl.when(jnp.logical_not(has_prev))
+    def _():
+        band[low, :] = jnp.zeros((WINDOW, 2 * k_cols), bf16)
+
+    @pl.when(jnp.logical_not(has_next))
+    def _():
+        band[high, :] = jnp.zeros((WINDOW, 2 * k_cols), bf16)
+
+    @pl.when(has_prev)
+    def _():
+        tail_copy.wait_recv()
+
+    @pl.when(has_next)
+    def _():
+        head_copy.wait_recv()
+
+    band_rows = rows + 2 * WINDOW
+    q_at = lax.broadcasted_iota(jnp.int32, (rows, band_rows), 0)
+    k_at = lax.broadcasted_iota(jnp.int32, (rows, band_rows), 1) - WINDOW
+    k_pos = k_at + s * rows
+    in_window = (
+        (jnp.abs(q_at - k_at) <= WINDOW) & (k_pos >= 0) & (k_pos < rows * count)
+    )
+    lane_at = lax.broadcasted_iota(jnp.int32, (8, LANES), 1)
+    sink_row = jnp.zeros((8, LANES), jnp.float32)
+    for kh in range(key_heads):
+        keys = band[:, kh * HEAD : (kh + 1) * HEAD]
+        values = band[:, k_cols + kh * HEAD : k_cols + (kh + 1) * HEAD]
+        key_sum = value_sum = None
+        for g in range(group):
+            h = kh * group + g
+            cols = slice(h * HEAD, (h + 1) * HEAD)
+            q, do = qs[:, cols], dos[:, cols]
+            scores = jnp.where(in_window, contract_cols(q, keys) * scaling, masked_score)
+            sink = sink_ref[0, h]
+            top = jnp.maximum(jnp.max(scores, axis=1, keepdims=True), sink)
+            e = jnp.exp(scores - top)
+            sink_e = jnp.exp(sink - top)
+            inverse = 1.0 / (jnp.sum(e, axis=1, keepdims=True) + sink_e)
+            p = e * inverse
+            p_low = p.astype(bf16)
+            attended = dot_nn(p_low, values).astype(bf16)
+            dots = jnp.sum(
+                do.astype(jnp.float32) * attended.astype(jnp.float32), axis=1, keepdims=True
+            )
+            ds = (p * (contract_cols(do, values) - dots)).astype(bf16)
+            acts_e[s, :, cols] = (dot_nn(ds, keys) * scaling).astype(bf16)
+            acts_e[s, :, q_cols + h * HEAD : q_cols + (h + 1) * HEAD] = attended
+            kg, vg = contract_rows(ds, q), contract_rows(p_low, do)
+            key_sum = kg if g == 0 else key_sum + kg
+            value_sum = vg if g == 0 else value_sum + vg
+            total = -jnp.sum(sink_e * inverse * dots)
+            sink_row = jnp.where(lane_at == h, total, sink_row)
+        bg[:, kh * HEAD : (kh + 1) * HEAD] = key_sum * scaling
+        bg[:, k_cols + kh * HEAD : k_cols + (kh + 1) * HEAD] = value_sum
+    sinks[s] = sink_row
+    ret_out[0] = bg[low, :].astype(bf16)
+    ret_out[1] = bg[high, :].astype(bf16)
+    to_prev = remote(ret_out.at[0], ret_in.at[0], ret_send.at[0], ret_recv.at[0], prev, t)
+    to_next = remote(ret_out.at[1], ret_in.at[1], ret_send.at[1], ret_recv.at[1], nxt, t)
+
+    @pl.when(has_prev)
+    def _():
+        to_prev.start()
+
+    @pl.when(has_next)
+    def _():
+        to_next.start()
+
+    acts = (acts_e, acts_l)
+    has_up, has_down = z < depth - 1, z > 0
+    up, down, other = (z + 1) % depth * 2 + x, (z + depth - 1) % depth * 2 + x, z * 2 + (1 - x)
+
+    def acts_copy(a, block, sems, dev):
+        ref = acts[a].at[block]
+        return remote(ref, ref, sems.at[a, block], acts_recv.at[a, block], dev, t)
+
+    def send_own(a):
+        acts_copy(a, s, cross_sem, other).start()
+
+        @pl.when(has_up)
+        def _():
+            acts_copy(a, s, up_sem, up).start()
+
+        @pl.when(has_down)
+        def _():
+            acts_copy(a, s, down_sem, down).start()
+
+    send_own(0)
+    sink_copies = []
+    for d in range(1, count):
+        sink_copies.append(
+            remote(
+                sinks.at[s], sinks.at[s], sink_send.at[d], sink_recv.at[d], (s + d) % count, t
+            )
+        )
+        sink_copies[-1].start()
+
+    tail, head = pl.ds(WINDOW + rows - WINDOW, WINDOW), pl.ds(WINDOW, WINDOW)
+
+    @pl.when(has_next)
+    def _():
+        to_prev.wait_recv()
+        bg[tail, :] = bg[tail, :] + ret_in[0].astype(jnp.float32)
+
+    @pl.when(has_prev)
+    def _():
+        to_next.wait_recv()
+        bg[head, :] = bg[head, :] + ret_in[1].astype(jnp.float32)
+
+    acts_l[s] = bg[mid, :].astype(bf16)
+    send_own(1)
+
+    qg = acts_e[s, :, :q_cols]
+    kg, vg = acts_l[s, :, :k_cols], acts_l[s, :, k_cols:]
+
+    def partial_for(slot):
+        span = pl.ds(pl.multiple_of(slot * feats, feats), feats)
+        return (
+            contract_cols(qg, wq[span, :])
+            + contract_cols(kg, wk[span, :])
+            + contract_cols(vg, wv[span, :])
+        ).astype(bf16)
+
+    rs_copies = []
+    for i, peer in enumerate((across, diag, partner)):
+        part[i] = partial_for(peer)
+        rs_copies.append(
+            remote(part.at[i], rs_in.at[i], rs_send.at[i], rs_recv.at[i], s, peer)
+        )
+        rs_copies[-1].start()
+
+    def forward(d):
+        for a in range(2):
+            lower, upper = (z + depth - d) % depth * 2 + x, (z + d) % depth * 2 + x
+
+            @pl.when(z >= d)
+            def _():
+                acts_copy(a, lower, up_sem, up).wait_recv()
+                acts_copy(a, lower, cross_sem, other).start()
+
+                @pl.when(has_up)
+                def _():
+                    acts_copy(a, lower, up_sem, up).start()
+
+            @pl.when(z + d < depth)
+            def _():
+                acts_copy(a, upper, down_sem, down).wait_recv()
+                acts_copy(a, upper, cross_sem, other).start()
+
+                @pl.when(has_down)
+                def _():
+                    acts_copy(a, upper, down_sem, down).start()
+
+    def consume(block, first=False):
+        early, late = acts_e[block], acts_l[block]
+        right = jnp.concatenate([early[:, :q_cols], late], axis=1)
+        left = jnp.concatenate([blk[i, block, 0] for i in range(tps)], axis=1)
+        grads = jnp.concatenate([blk[i, block, 1] for i in range(tps)], axis=1)
+        term = contract_rows(left, right)
+        out_term = contract_rows(early[:, q_cols:], grads)
+        pieces = (
+            (gq_ref, term[:, :q_cols]),
+            (gk_ref, term[:, q_cols : q_cols + k_cols]),
+            (gv_ref, term[:, q_cols + k_cols :]),
+            (go_ref, out_term),
+        )
+        for ref, value in pieces:
+            ref[...] = value if first else ref[...] + value
+
+    def consume_crossed(block_z):
+        block = block_z * 2 + (1 - x)
+        for a in range(2):
+            acts_copy(a, block, cross_sem, other).wait_recv()
+        consume(block)
+
+    def consume_far(d):
+        lower, upper = (z + depth - d) % depth, (z + d) % depth
+
+        @pl.when(z >= d)
+        def _():
+            consume(lower * 2 + x)
+            consume_crossed(lower)
+
+        @pl.when(z + d < depth)
+        def _():
+            consume(upper * 2 + x)
+            consume_crossed(upper)
+
+    own_block.wait()
+    for copy in a2a:
+        copy.wait_recv()
+    blk_across = remote(blk.at[t], blk.at[t], blk_send.at[0], blk_recv.at[0], s, across)
+    blk_partner = remote(blk.at[t], blk.at[t], blk_send.at[1], blk_recv.at[1], s, partner)
+    blk_relay = remote(blk.at[across], blk.at[across], blk_send.at[2], blk_recv.at[2], s, partner)
+    blk_across.start()
+    blk_partner.start()
+    forward(1)
+    mine = partial_for(t)
+    blk_across.wait_recv()
+    blk_relay.start()
+    blk_partner.wait_recv()
+    blk_relay.wait_recv()
+    consume(s, True)
+    forward(2)
+    consume_crossed(z)
+    for d in range(1, depth):
+        if d + 2 < depth:
+            forward(d + 2)
+        consume_far(d)
+    for copy in rs_copies:
+        copy.wait_recv()
+    total = mine.astype(jnp.float32)
+    for i in range(3):
+        total = total + rs_in[i].astype(jnp.float32)
+    ig_ref[...] = total.astype(bf16)
+    for copy in sink_copies:
+        copy.wait_recv()
+    sink_total = sinks[0]
+    for i in range(1, count):
+        sink_total = sink_total + sinks[i]
+    sg_ref[...] = sink_total
+
+    for copy in to_across + to_partner + relay + a2a + rs_copies + sink_copies:
+        copy.wait_send()
+    for copy in (blk_across, blk_partner, blk_relay):
+        copy.wait_send()
+
+    @pl.when(has_next)
+    def _():
+        tail_copy.wait_send()
+        to_next.wait_send()
+
+    @pl.when(has_prev)
+    def _():
+        head_copy.wait_send()
+        to_prev.wait_send()
+
+    for a in range(2):
+        acts_copy(a, s, cross_sem, other).wait_send()
+
+        @pl.when(has_up)
+        def _():
+            acts_copy(a, s, up_sem, up).wait_send()
+
+        @pl.when(has_down)
+        def _():
+            acts_copy(a, s, down_sem, down).wait_send()
+
+        for d in range(1, depth):
+            lower, upper = (z + depth - d) % depth * 2 + x, (z + d) % depth * 2 + x
+
+            @pl.when(z >= d)
+            def _():
+                acts_copy(a, lower, cross_sem, other).wait_send()
+
+                @pl.when(has_up)
+                def _():
+                    acts_copy(a, lower, up_sem, up).wait_send()
+
+            @pl.when(z + d < depth)
+            def _():
+                acts_copy(a, upper, cross_sem, other).wait_send()
+
+                @pl.when(has_down)
+                def _():
+                    acts_copy(a, upper, down_sem, down).wait_send()
+
+
+def fused_device(
+    layer_input, output_grad, query_weight, key_weight, value_weight, out_weight, sink_logit
+):
+    bf16, f32 = jnp.bfloat16, jnp.float32
+    count, tps = lax.axis_size("sp"), lax.axis_size("tp")
+    rows, feats = layer_input.shape
+    width = query_weight.shape[0]
+    q_cols, k_cols = query_weight.shape[1], key_weight.shape[1]
+    block_cols = width // count
+    vmem = pl.BlockSpec(memory_space=pltpu.VMEM)
+    hbm = pl.BlockSpec(memory_space=pl.ANY)
+    dma = pltpu.SemaphoreType.DMA
+    outs = pl.pallas_call(
+        layer_kernel,
+        out_shape=(
+            jax.ShapeDtypeStruct((rows, feats), bf16),
+            jax.ShapeDtypeStruct((block_cols, q_cols), f32),
+            jax.ShapeDtypeStruct((block_cols, k_cols), f32),
+            jax.ShapeDtypeStruct((block_cols, k_cols), f32),
+            jax.ShapeDtypeStruct((q_cols, block_cols), f32),
+            jax.ShapeDtypeStruct((8, LANES), f32),
+        ),
+        in_specs=[vmem, vmem, hbm, hbm, hbm, hbm, pl.BlockSpec(memory_space=pltpu.SMEM)],
+        out_specs=(vmem,) * 6,
+        scratch_shapes=[
+            pltpu.VMEM(query_weight.shape, bf16),
+            pltpu.VMEM(key_weight.shape, bf16),
+            pltpu.VMEM(value_weight.shape, bf16),
+            pltpu.VMEM(out_weight.shape, bf16),
+            pltpu.VMEM((tps, 2, rows, feats), bf16),
+            pltpu.VMEM((rows, 2 * q_cols + 2 * k_cols), f32),
+            pltpu.VMEM((rows, q_cols), bf16),
+            pltpu.VMEM((rows, q_cols), bf16),
+            pltpu.VMEM((rows + 2 * WINDOW, 2 * k_cols), bf16),
+            pltpu.VMEM((rows + 2 * WINDOW, 2 * k_cols), f32),
+            pltpu.VMEM((2, WINDOW, 2 * k_cols), bf16),
+            pltpu.VMEM((2, WINDOW, 2 * k_cols), bf16),
+            pltpu.VMEM((tps, count, 2, rows, LANES), bf16),
+            pltpu.VMEM((count, rows, 2 * q_cols), bf16),
+            pltpu.VMEM((count, rows, 2 * k_cols), bf16),
+            pltpu.VMEM((3, rows, feats), bf16),
+            pltpu.VMEM((3, rows, feats), bf16),
+            pltpu.VMEM((count, 8, LANES), f32),
+            dma((4,)), dma((3,)), dma((3, 2)), dma((3, 2)),
+            dma((2,)), dma((2,)), dma((2,)), dma((2,)),
+            dma((count,)), dma((count,)), dma((3,)), dma((3,)),
+            dma((2, count)), dma((2, count)), dma((2, count)), dma((2, count)),
+            dma((3,)), dma((3,)), dma((count,)), dma((count,)),
+        ],
+        compiler_params=pltpu.CompilerParams(
+            collective_id=0, has_side_effects=True, vmem_limit_bytes=VMEM_BYTES
+        ),
+        name="layer",
+    )(
+        layer_input, output_grad, query_weight, key_weight, value_weight, out_weight,
+        sink_logit.reshape(1, -1),
+    )
+    return outs[:5] + (outs[5][0, : sink_logit.shape[0]],)
+
+
+def fits_kernel(mesh, layer_width):
+    count, tps = mesh.shape["sp"], mesh.shape["tp"]
+    return tps == 4 and count % 8 == 0 and layer_width == count * tps * LANES
+
+
 def solution(mesh):
     placed = (
         P("sp", "tp"),
@@ -175,17 +664,23 @@
         P("tp", None),
         P("tp"),
     )
-    return jax.shard_map(
-        per_device,
-        mesh=mesh,
-        in_specs=placed,
-        out_specs=(
-            P("sp", "tp"),
-            P("sp", "tp"),
-            P("sp", "tp"),
-            P("sp", "tp"),
-            P("tp", "sp"),
-            P("tp"),
-        ),
-        check_vma=False,
-    )
+
+    def sharded(*arrays):
+        width = arrays[0].shape[1]
+        body = fused_device if fits_kernel(mesh, width) else per_device
+        return jax.shard_map(
+            body,
+            mesh=mesh,
+            in_specs=placed,
+            out_specs=(
+                P("sp", "tp"),
+                P("sp", "tp"),
+                P("sp", "tp"),
+                P("sp", "tp"),
+                P("tp", "sp"),
+                P("tp"),
+            ),
+            check_vma=False,
+        )(*arrays)
+
+    return sharded

time: 248 us -> 112 us (0.45)
  Pallas kernels: 0 us -> 101 us
  waiting for transfers between devices: 94.8 us -> 0 us
  blocking collectives: 47.5 us -> 0 us
  matrix products: 34.4 us -> 0 us
  starting transfers between devices: 21.1 us -> 0 us
  local copies, waits for them, and re-layouts: 29.1 us -> 9.97 us
  between operations: 14 us -> 0.65 us
  other arithmetic: 5.94 us -> 0 us
    pallas_call x0 -> x1, Pallas kernels: none -> 101 us  [fused_device(): pl.pallas_call(layer_kernel, out_shape=(jax.ShapeDtypeStruct((rows, feats...]
    psum x1 -> x0, blocking collectives: 47.5 us -> none  [per_device(): sink_grad = lax.psum(sink_part, 'sp')]
    all_gather x4 -> x0, waiting for transfers between devices: 36.8 us -> none  [the longest x1 20.2 us: per_device(): lax.all_gather(layer_input, 'tp', axis=1, tiled=True)]
    dot_general x17 -> x0, matrix products: 34.4 us -> none  [the longest x4 12.5 us: contract_rows(): lax.dot_general(left, right, (((0,), (0,)), ((), ())), preferred_element_...]
    all_to_all x2 -> x0, waiting for transfers between devices: 33.8 us -> none  [the longest x1 33.8 us: per_device(): input_block = lax.all_to_all(whole_input, 'sp', 1, 0, tiled=True)]
    reduce_scatter x1 -> x0, waiting for transfers between devices: 18.6 us -> none  [per_device(): lax.psum_scatter(partials.astype(jnp.bfloat16), 'tp', scatter_dimension=1...]
    ppermute x4 -> x0, starting transfers between devices: 11.1 us -> none  [the longest x2 5.85 us: passed_along(): lax.ppermute(value, axis, [(source, source + steps) for source in range(i...]
    reshape x6 -> x0, local copies, waits for them, and re-layouts: 9.88 us -> none  [the longest x1 1.67 us: per_device(): band_values = band[:, key_cols:].reshape(band_rows, key_heads, HEAD)]
  transfers between devices with their start and end apart: 11 -> 0, of which waited for: 7 -> 0; matrix products, arithmetic and copies ran while one was open for 21% -> 0% of each run, Pallas kernels for 0% -> 0%
where the time goes in v2:
time: 112 us
  Pallas kernels  101 us (90%)
  local copies, waits for them, and re-layouts  9.97 us (9%)
    pallas_call x1, Pallas kernels, fused_device(): pl.pallas_call(layer_kernel, out_shape=(jax.ShapeDtypeStruct((rows, feats...  101 us
    unnamed x7, local copies, waits for them, and re-layouts  8.69 us

profile of v2, /device:TPU:0, one launch (start us, length us, event | category | flops | bytes accessed | tf_op | source)
XLA Modules:
  0.0 112.0 jit_solution(6790107687602160595)
XLA Ops:
  0.6 101.3 %layer.1 = (bf16[160,1024]{1,0:T(8,128)(2,1)}, f32[512,512]{1,0:T(8,128)}, f32[512,256]{1,0:T(8,128)}, f32[512,256]{1,0:T(8,128)}, f32[512,512]{1,0:T(8,128)}, /*index=5*/f32[8,128]{1,0:T(8,128)}) custom-call(bf16[160,1024]{1,0:T(8,128)(2,1)} %x_ref.1, bf16[160,1024]{1,0:T(8,128)(2,1)} %g_ref.1, bf16[4096,512]{1,0:T(8,128)(2,1)} %wq_hbm.1, ...), custom_call_target="tpu_custom_call" | custom-call | tf_op jit(solution)/shard_map/layer/pallas_call | solution.py:604
  102.0 0.0 copy-start
  102.0 1.3 %slice_bitcast_fusion = f32[4]{0:T(128)} fusion(f32[8,128]{1,0:T(8,128)} %get-tuple-element.17), kind=kLoop, calls=%fused_computation | loop fusion | bytes 32 | tf_op jit(solution)/shard_map/squeeze | solution.py:649
  103.3 1.7 %copy.18 = bf16[160,1024]{1,0:T(8,128)(2,1)} copy(bf16[160,1024]{1,0:T(8,128)(2,1)} %get-tuple-element.24) | data formatting | bytes 655360
  105.0 2.3 %copy.19 = f32[512,512]{1,0:T(8,128)} copy(f32[512,512]{1,0:T(8,128)} %get-tuple-element.25) | data formatting | bytes 2097152
  107.2 1.9 %copy.20 = f32[512,256]{1,0:T(8,128)} copy(f32[512,256]{1,0:T(8,128)} %get-tuple-element.26) | data formatting | bytes 1048576
  109.1 1.9 %copy.21 = f32[512,256]{1,0:T(8,128)} copy(f32[512,256]{1,0:T(8,128)} %get-tuple-element.27) | data formatting | bytes 1048576
  111.0 0.0 copy-done
  111.0 1.0 copy.22
Async XLA Ops:
  102.0 9.0 %copy-start = (f32[512,512]{1,0:T(8,128)S(1)}, f32[512,512]{1,0:T(8,128)}, u32[]{:S(2)}) copy-start(f32[512,512]{1,0:T(8,128)} %get-tuple-element.28) | copy-start | bytes 3145732

commit v3 on v2

--- a/solution.py
+++ b/solution.py
@@ -299,6 +299,27 @@
     def _():
         head_copy.start()
 
+    own_blocks, a2a = [], []
+
+    def columns(a, j):
+        lane = (j % per_slot) * block_cols + t * LANES
+        return xg.at[j // per_slot, a, :, pl.ds(pl.multiple_of(lane, LANES), LANES)]
+
+    def send_columns(a):
+        own_blocks.append(
+            pltpu.make_async_copy(columns(a, s), blk.at[t, s, a], own_sem.at[2 + a])
+        )
+        own_blocks[-1].start()
+        for d in range(1, count):
+            j = (s + d) % count
+            a2a.append(
+                remote(
+                    columns(a, j), blk.at[t, s, a], a2a_send.at[a, d], a2a_recv.at[a, d], j, t
+                )
+            )
+            a2a[-1].start()
+
+    send_columns(0)
     to_across[1].wait_recv()
     relay[1].start()
     project_grad(across, False)
@@ -306,19 +327,7 @@
     project_grad(diag, False)
     dos[...] = acc[:, q_cols + 2 * k_cols :].astype(bf16)
 
-    def a2a_source(j):
-        lane = (j % per_slot) * block_cols + t * LANES
-        return xg.at[j // per_slot, :, :, pl.ds(pl.multiple_of(lane, LANES), LANES)]
-
-    own_block = pltpu.make_async_copy(a2a_source(s), blk.at[t, s], own_sem.at[2])
-    own_block.start()
-    a2a = []
-    for d in range(1, count):
-        j = (s + d) % count
-        a2a.append(
-            remote(a2a_source(j), blk.at[t, s], a2a_send.at[d], a2a_recv.at[d], j, t)
-        )
-        a2a[-1].start()
+    send_columns(1)
 
     @pl.when(jnp.logical_not(has_prev))
     def _():
@@ -433,6 +442,15 @@
     acts_l[s] = bg[mid, :].astype(bf16)
     send_own(1)
 
+    for copy in own_blocks:
+        copy.wait()
+    for copy in a2a:
+        copy.wait_recv()
+    blk_across = remote(blk.at[t], blk.at[t], blk_send.at[0], blk_recv.at[0], s, across)
+    blk_partner = remote(blk.at[t], blk.at[t], blk_send.at[1], blk_recv.at[1], s, partner)
+    blk_relay = remote(blk.at[across], blk.at[across], blk_send.at[2], blk_recv.at[2], s, partner)
+    blk_across.start()
+    blk_partner.start()
     qg = acts_e[s, :, :q_cols]
     kg, vg = acts_l[s, :, :k_cols], acts_l[s, :, k_cols:]
 
@@ -509,26 +527,17 @@
             consume(upper * 2 + x)
             consume_crossed(upper)
 
-    own_block.wait()
-    for copy in a2a:
-        copy.wait_recv()
-    blk_across = remote(blk.at[t], blk.at[t], blk_send.at[0], blk_recv.at[0], s, across)
-    blk_partner = remote(blk.at[t], blk.at[t], blk_send.at[1], blk_recv.at[1], s, partner)
-    blk_relay = remote(blk.at[across], blk.at[across], blk_send.at[2], blk_recv.at[2], s, partner)
-    blk_across.start()
-    blk_partner.start()
+    mine = partial_for(t)
     forward(1)
-    mine = partial_for(t)
     blk_across.wait_recv()
     blk_relay.start()
+    for d in range(2, depth):
+        forward(d)
     blk_partner.wait_recv()
     blk_relay.wait_recv()
     consume(s, True)
-    forward(2)
     consume_crossed(z)
     for d in range(1, depth):
-        if d + 2 < depth:
-            forward(d + 2)
         consume_far(d)
     for copy in rs_copies:
         copy.wait_recv()
@@ -587,6 +596,21 @@
                 @pl.when(has_down)
                 def _():
                     acts_copy(a, upper, down_sem, down).wait_send()
+
+
+def store_kernel(*refs):
+    ins, sink_in, outs, sink_out = refs[:5], refs[5], refs[6:11], refs[11]
+    held, in_sem, out_sem = refs[12:17], refs[17], refs[18]
+    loads = [pltpu.make_async_copy(ins[i], held[i], in_sem.at[i]) for i in range(5)]
+    stores = [pltpu.make_async_copy(held[i], outs[i], out_sem.at[i]) for i in range(5)]
+    for load in loads:
+        load.start()
+    sink_out[...] = sink_in[0:1, : sink_out.shape[1]]
+    for load, store in zip(loads, stores):
+        load.wait()
+        store.start()
+    for store in stores:
+        store.wait()
 
 
 def fused_device(
@@ -632,9 +656,9 @@
             pltpu.VMEM((3, rows, feats), bf16),
             pltpu.VMEM((3, rows, feats), bf16),
             pltpu.VMEM((count, 8, LANES), f32),
-            dma((4,)), dma((3,)), dma((3, 2)), dma((3, 2)),
+            dma((4,)), dma((4,)), dma((3, 2)), dma((3, 2)),
             dma((2,)), dma((2,)), dma((2,)), dma((2,)),
-            dma((count,)), dma((count,)), dma((3,)), dma((3,)),
+            dma((2, count)), dma((2, count)), dma((3,)), dma((3,)),
             dma((2, count)), dma((2, count)), dma((2, count)), dma((2, count)),
             dma((3,)), dma((3,)), dma((count,)), dma((count,)),
         ],
@@ -646,7 +670,18 @@
         layer_input, output_grad, query_weight, key_weight, value_weight, out_weight,
         sink_logit.reshape(1, -1),
     )
-    return outs[:5] + (outs[5][0, : sink_logit.shape[0]],)
+    kept = [jax.ShapeDtypeStruct(out.shape, out.dtype) for out in outs[:5]]
+    stored = pl.pallas_call(
+        store_kernel,
+        out_shape=(*kept, jax.ShapeDtypeStruct((1, sink_logit.shape[0]), f32)),
+        in_specs=[hbm] * 5 + [vmem],
+        out_specs=(hbm,) * 5 + (vmem,),
+        scratch_shapes=[pltpu.VMEM(out.shape, out.dtype) for out in kept]
+        + [dma((5,)), dma((5,))],
+        compiler_params=pltpu.CompilerParams(vmem_limit_bytes=VMEM_BYTES),
+        name="store",
+    )(*outs)
+    return tuple(stored[:5]) + (stored[5].reshape(-1),)
 
 
 def fits_kernel(mesh, layer_width):

time: 112 us -> 89.9 us (0.80); the launches traced: 112 us -> 88.3 us
  Pallas kernels: 101 us -> 87.5 us
  local copies, waits for them, and re-layouts: 9.97 us -> 0 us
    pallas_call x1, Pallas kernels: 101 us -> 83.2 us  [fused_device(): pl.pallas_call(layer_kernel, out_shape=(jax.ShapeDtypeStruct((rows, feats...]
    unnamed x7 -> x0, local copies, waits for them, and re-layouts: 8.69 us -> none
    pallas_call x0 -> x1, Pallas kernels: none -> 4.33 us  [fused_device(): pl.pallas_call(store_kernel, out_shape=(*kept, jax.ShapeDtypeStruct((1, s...]
    squeeze x1 -> x0, local copies, waits for them, and re-layouts: 1.28 us -> none  [fused_device(): return outs[:5] + (outs[5][0, :sink_logit.shape[0]],)]
where the time goes in v3:
time: 89.9 us; the launch traced here: 88.3 us
  Pallas kernels  87.5 us (97%)
    pallas_call x1, Pallas kernels, fused_device(): pl.pallas_call(layer_kernel, out_shape=(jax.ShapeDtypeStruct((rows, feats...  83.2 us
    pallas_call x1, Pallas kernels, fused_device(): pl.pallas_call(store_kernel, out_shape=(*kept, jax.ShapeDtypeStruct((1, s...  4.33 us

profile of v3, /device:TPU:0, one launch (start us, length us, event | category | flops | bytes accessed | tf_op | source)
XLA Modules:
  0.0 88.3 jit_solution(10444675239751622547)
XLA Ops:
  0.6 83.2 %layer.1 = (bf16[160,1024]{1,0:T(8,128)(2,1)}, f32[512,512]{1,0:T(8,128)}, f32[512,256]{1,0:T(8,128)}, f32[512,256]{1,0:T(8,128)}, f32[512,512]{1,0:T(8,128)}, /*index=5*/f32[8,128]{1,0:T(8,128)}) custom-call(bf16[160,1024]{1,0:T(8,128)(2,1)} %x_ref.1, bf16[160,1024]{1,0:T(8,128)(2,1)} %g_ref.1, bf16[4096,512]{1,0:T(8,128)(2,1)} %wq_hbm.1, ...), custom_call_target="tpu_custom_call" | custom-call | tf_op jit(solution)/shard_map/layer/pallas_call | solution.py:628
  83.8 4.3 %store.1 = (bf16[160,1024]{1,0:T(8,128)(2,1)}, f32[512,512]{1,0:T(8,128)}, f32[512,256]{1,0:T(8,128)}, f32[512,256]{1,0:T(8,128)}, f32[512,512]{1,0:T(8,128)}, /*index=5*/f32[1,4]{1,0:T(1,128)}) custom-call(bf16[160,1024]{1,0:T(8,128)(2,1)} %get-tuple-element.18.refs_0_, f32[512,512]{1,0:T(8,128)} %get-tuple-element.19.refs_1_, ...), custom_call_target="tpu_custom_call" | custom-call | tf_op jit(solution)/shard_map/store/pallas_call | solution.py:674

commit v4 on v3

--- a/solution.py
+++ b/solution.py
@@ -182,7 +182,7 @@
     x_ref, g_ref, wq_hbm, wk_hbm, wv_hbm, wo_hbm, sink_ref,
     ig_ref, gq_ref, gk_ref, gv_ref, go_ref, sg_ref,
     wq, wk, wv, wo, xg, acc, qs, dos, band, bg, ret_out, ret_in,
-    blk, acts_e, acts_l, part, rs_in, sinks,
+    blk, acts, probs, part, rs_in, sinks,
     w_sem, own_sem, ag_send, ag_recv, halo_send, halo_recv, ret_send, ret_recv,
     a2a_send, a2a_recv, blk_send, blk_recv, up_sem, down_sem, cross_sem, acts_recv,
     rs_send, rs_recv, sink_send, sink_recv,
@@ -320,6 +320,85 @@
             a2a[-1].start()
 
     send_columns(0)
+    @pl.when(jnp.logical_not(has_prev))
+    def _():
+        band[low, :] = jnp.zeros((WINDOW, 2 * k_cols), bf16)
+
+    @pl.when(jnp.logical_not(has_next))
+    def _():
+        band[high, :] = jnp.zeros((WINDOW, 2 * k_cols), bf16)
+
+    @pl.when(has_prev)
+    def _():
+        tail_copy.wait_recv()
+
+    @pl.when(has_next)
+    def _():
+        head_copy.wait_recv()
+
+    band_rows = rows + 2 * WINDOW
+    q_at = lax.broadcasted_iota(jnp.int32, (rows, band_rows), 0)
+    k_at = lax.broadcasted_iota(jnp.int32, (rows, band_rows), 1) - WINDOW
+    k_pos = k_at + s * rows
+    in_window = (
+        (jnp.abs(q_at - k_at) <= WINDOW) & (k_pos >= 0) & (k_pos < rows * count)
+    )
+    sink_shares = []
+    for h in range(key_heads * group):
+        kh = h // group
+        cols = slice(h * HEAD, (h + 1) * HEAD)
+        keys = band[:, kh * HEAD : (kh + 1) * HEAD]
+        values = band[:, k_cols + kh * HEAD : k_cols + (kh + 1) * HEAD]
+        scores = jnp.where(in_window, contract_cols(qs[:, cols], keys) * scaling, masked_score)
+        sink = sink_ref[0, h]
+        top = jnp.maximum(jnp.max(scores, axis=1, keepdims=True), sink)
+        e = jnp.exp(scores - top)
+        sink_e = jnp.exp(sink - top)
+        inverse = 1.0 / (jnp.sum(e, axis=1, keepdims=True) + sink_e)
+        p = e * inverse
+        probs[h] = p
+        sink_shares.append(sink_e * inverse)
+        acts[0, s, :, cols] = dot_nn(p.astype(bf16), values).astype(bf16)
+    has_up, has_down = z < depth - 1, z > 0
+    up, down, other = (z + 1) % depth * 2 + x, (z + depth - 1) % depth * 2 + x, z * 2 + (1 - x)
+
+    def acts_copy(a, block, sems, dev):
+        ref = acts.at[a, block]
+        return remote(ref, ref, sems.at[a, block], acts_recv.at[a, block], dev, t)
+
+    def send_own(a):
+        acts_copy(a, s, cross_sem, other).start()
+
+        @pl.when(has_up)
+        def _():
+            acts_copy(a, s, up_sem, up).start()
+
+        @pl.when(has_down)
+        def _():
+            acts_copy(a, s, down_sem, down).start()
+
+    def forward(d, a):
+        lower, upper = (z + depth - d) % depth * 2 + x, (z + d) % depth * 2 + x
+
+        @pl.when(z >= d)
+        def _():
+            acts_copy(a, lower, up_sem, up).wait_recv()
+            acts_copy(a, lower, cross_sem, other).start()
+
+            @pl.when(has_up)
+            def _():
+                acts_copy(a, lower, up_sem, up).start()
+
+        @pl.when(z + d < depth)
+        def _():
+            acts_copy(a, upper, down_sem, down).wait_recv()
+            acts_copy(a, upper, cross_sem, other).start()
+
+            @pl.when(has_down)
+            def _():
+                acts_copy(a, upper, down_sem, down).start()
+
+    send_own(0)
     to_across[1].wait_recv()
     relay[1].start()
     project_grad(across, False)
@@ -329,29 +408,6 @@
 
     send_columns(1)
 
-    @pl.when(jnp.logical_not(has_prev))
-    def _():
-        band[low, :] = jnp.zeros((WINDOW, 2 * k_cols), bf16)
-
-    @pl.when(jnp.logical_not(has_next))
-    def _():
-        band[high, :] = jnp.zeros((WINDOW, 2 * k_cols), bf16)
-
-    @pl.when(has_prev)
-    def _():
-        tail_copy.wait_recv()
-
-    @pl.when(has_next)
-    def _():
-        head_copy.wait_recv()
-
-    band_rows = rows + 2 * WINDOW
-    q_at = lax.broadcasted_iota(jnp.int32, (rows, band_rows), 0)
-    k_at = lax.broadcasted_iota(jnp.int32, (rows, band_rows), 1) - WINDOW
-    k_pos = k_at + s * rows
-    in_window = (
-        (jnp.abs(q_at - k_at) <= WINDOW) & (k_pos >= 0) & (k_pos < rows * count)
-    )
     lane_at = lax.broadcasted_iota(jnp.int32, (8, LANES), 1)
     sink_row = jnp.zeros((8, LANES), jnp.float32)
     for kh in range(key_heads):
@@ -361,26 +417,17 @@
         for g in range(group):
             h = kh * group + g
             cols = slice(h * HEAD, (h + 1) * HEAD)
-            q, do = qs[:, cols], dos[:, cols]
-            scores = jnp.where(in_window, contract_cols(q, keys) * scaling, masked_score)
-            sink = sink_ref[0, h]
-            top = jnp.maximum(jnp.max(scores, axis=1, keepdims=True), sink)
-            e = jnp.exp(scores - top)
-            sink_e = jnp.exp(sink - top)
-            inverse = 1.0 / (jnp.sum(e, axis=1, keepdims=True) + sink_e)
-            p = e * inverse
-            p_low = p.astype(bf16)
-            attended = dot_nn(p_low, values).astype(bf16)
+            q, do, p = qs[:, cols], dos[:, cols], probs[h]
+            attended = acts[0, s, :, cols]
             dots = jnp.sum(
                 do.astype(jnp.float32) * attended.astype(jnp.float32), axis=1, keepdims=True
             )
             ds = (p * (contract_cols(do, values) - dots)).astype(bf16)
-            acts_e[s, :, cols] = (dot_nn(ds, keys) * scaling).astype(bf16)
-            acts_e[s, :, q_cols + h * HEAD : q_cols + (h + 1) * HEAD] = attended
-            kg, vg = contract_rows(ds, q), contract_rows(p_low, do)
+            acts[1, s, :, cols] = (dot_nn(ds, keys) * scaling).astype(bf16)
+            kg, vg = contract_rows(ds, q), contract_rows(p.astype(bf16), do)
             key_sum = kg if g == 0 else key_sum + kg
             value_sum = vg if g == 0 else value_sum + vg
-            total = -jnp.sum(sink_e * inverse * dots)
+            total = -jnp.sum(sink_shares[h] * dots)
             sink_row = jnp.where(lane_at == h, total, sink_row)
         bg[:, kh * HEAD : (kh + 1) * HEAD] = key_sum * scaling
         bg[:, k_cols + kh * HEAD : k_cols + (kh + 1) * HEAD] = value_sum
@@ -398,26 +445,7 @@
     def _():
         to_next.start()
 
-    acts = (acts_e, acts_l)
-    has_up, has_down = z < depth - 1, z > 0
-    up, down, other = (z + 1) % depth * 2 + x, (z + depth - 1) % depth * 2 + x, z * 2 + (1 - x)
-
-    def acts_copy(a, block, sems, dev):
-        ref = acts[a].at[block]
-        return remote(ref, ref, sems.at[a, block], acts_recv.at[a, block], dev, t)
-
-    def send_own(a):
-        acts_copy(a, s, cross_sem, other).start()
-
-        @pl.when(has_up)
-        def _():
-            acts_copy(a, s, up_sem, up).start()
-
-        @pl.when(has_down)
-        def _():
-            acts_copy(a, s, down_sem, down).start()
-
-    send_own(0)
+    send_own(1)
     sink_copies = []
     for d in range(1, count):
         sink_copies.append(
@@ -439,8 +467,9 @@
         to_next.wait_recv()
         bg[head, :] = bg[head, :] + ret_in[1].astype(jnp.float32)
 
-    acts_l[s] = bg[mid, :].astype(bf16)
-    send_own(1)
+    forward(1, 0)
+    acts[2, s] = bg[mid, :].astype(bf16)
+    send_own(2)
 
     for copy in own_blocks:
         copy.wait()
@@ -451,8 +480,8 @@
     blk_relay = remote(blk.at[across], blk.at[across], blk_send.at[2], blk_recv.at[2], s, partner)
     blk_across.start()
     blk_partner.start()
-    qg = acts_e[s, :, :q_cols]
-    kg, vg = acts_l[s, :, :k_cols], acts_l[s, :, k_cols:]
+    qg = acts[1, s]
+    kg, vg = acts[2, s, :, :k_cols], acts[2, s, :, k_cols:]
 
     def partial_for(slot):
         span = pl.ds(pl.multiple_of(slot * feats, feats), feats)
@@ -470,35 +499,12 @@
         )
         rs_copies[-1].start()
 
-    def forward(d):
-        for a in range(2):
-            lower, upper = (z + depth - d) % depth * 2 + x, (z + d) % depth * 2 + x
-
-            @pl.when(z >= d)
-            def _():
-                acts_copy(a, lower, up_sem, up).wait_recv()
-                acts_copy(a, lower, cross_sem, other).start()
-
-                @pl.when(has_up)
-                def _():
-                    acts_copy(a, lower, up_sem, up).start()
-
-            @pl.when(z + d < depth)
-            def _():
-                acts_copy(a, upper, down_sem, down).wait_recv()
-                acts_copy(a, upper, cross_sem, other).start()
-
-                @pl.when(has_down)
-                def _():
-                    acts_copy(a, upper, down_sem, down).start()
-
     def consume(block, first=False):
-        early, late = acts_e[block], acts_l[block]
-        right = jnp.concatenate([early[:, :q_cols], late], axis=1)
+        right = jnp.concatenate([acts[1, block], acts[2, block]], axis=1)
         left = jnp.concatenate([blk[i, block, 0] for i in range(tps)], axis=1)
         grads = jnp.concatenate([blk[i, block, 1] for i in range(tps)], axis=1)
         term = contract_rows(left, right)
-        out_term = contract_rows(early[:, q_cols:], grads)
+        out_term = contract_rows(acts[0, block], grads)
         pieces = (
             (gq_ref, term[:, :q_cols]),
             (gk_ref, term[:, q_cols : q_cols + k_cols]),
@@ -510,7 +516,7 @@
 
     def consume_crossed(block_z):
         block = block_z * 2 + (1 - x)
-        for a in range(2):
+        for a in range(3):
             acts_copy(a, block, cross_sem, other).wait_recv()
         consume(block)
 
@@ -528,11 +534,12 @@
             consume_crossed(upper)
 
     mine = partial_for(t)
-    forward(1)
+    forward(1, 1)
     blk_across.wait_recv()
     blk_relay.start()
-    for d in range(2, depth):
-        forward(d)
+    later = [(d, a) for d in range(1, depth) for a in range(3) if d > 1 or a > 1]
+    for d, a in sorted(later, key=sum):
+        forward(d, a)
     blk_partner.wait_recv()
     blk_relay.wait_recv()
     consume(s, True)
@@ -567,7 +574,7 @@
         head_copy.wait_send()
         to_prev.wait_send()
 
-    for a in range(2):
+    for a in range(3):
         acts_copy(a, s, cross_sem, other).wait_send()
 
         @pl.when(has_up)
@@ -651,15 +658,15 @@
             pltpu.VMEM((2, WINDOW, 2 * k_cols), bf16),
             pltpu.VMEM((2, WINDOW, 2 * k_cols), bf16),
             pltpu.VMEM((tps, count, 2, rows, LANES), bf16),
-            pltpu.VMEM((count, rows, 2 * q_cols), bf16),
-            pltpu.VMEM((count, rows, 2 * k_cols), bf16),
+            pltpu.VMEM((3, count, rows, q_cols), bf16),
+            pltpu.VMEM((q_cols // HEAD, rows, rows + 2 * WINDOW), f32),
             pltpu.VMEM((3, rows, feats), bf16),
             pltpu.VMEM((3, rows, feats), bf16),
             pltpu.VMEM((count, 8, LANES), f32),
             dma((4,)), dma((4,)), dma((3, 2)), dma((3, 2)),
             dma((2,)), dma((2,)), dma((2,)), dma((2,)),
             dma((2, count)), dma((2, count)), dma((3,)), dma((3,)),
-            dma((2, count)), dma((2, count)), dma((2, count)), dma((2, count)),
+            dma((3, count)), dma((3, count)), dma((3, count)), dma((3, count)),
             dma((3,)), dma((3,)), dma((count,)), dma((count,)),
         ],
         compiler_params=pltpu.CompilerParams(

time: 89.9 us -> 95.6 us (1.063); the launches traced: 88.3 us -> 95.4 us
  Pallas kernels: 87.5 us -> 94.6 us
    pallas_call x1, Pallas kernels: 83.2 us -> 90.3 us  [fused_device(): pl.pallas_call(layer_kernel, out_shape=(jax.ShapeDtypeStruct((rows, feats...]
where the time goes in v4:
time: 95.6 us; the launch traced here: 95.4 us
  Pallas kernels  94.6 us (99%)
    pallas_call x1, Pallas kernels, fused_device(): pl.pallas_call(layer_kernel, out_shape=(jax.ShapeDtypeStruct((rows, feats...  90.3 us
    pallas_call x1, Pallas kernels, fused_device(): pl.pallas_call(store_kernel, out_shape=(*kept, jax.ShapeDtypeStruct((1, s...  4.33 us

profile of v4, /device:TPU:0, one launch (start us, length us, event | category | flops | bytes accessed | tf_op | source)
XLA Modules:
  0.0 95.4 jit_solution(18293356659661671661)
XLA Ops:
  0.6 90.3 %layer.1 = (bf16[160,1024]{1,0:T(8,128)(2,1)}, f32[512,512]{1,0:T(8,128)}, f32[512,256]{1,0:T(8,128)}, f32[512,256]{1,0:T(8,128)}, f32[512,512]{1,0:T(8,128)}, /*index=5*/f32[8,128]{1,0:T(8,128)}) custom-call(bf16[160,1024]{1,0:T(8,128)(2,1)} %x_ref.1, bf16[160,1024]{1,0:T(8,128)(2,1)} %g_ref.1, bf16[4096,512]{1,0:T(8,128)(2,1)} %wq_hbm.1, ...), custom_call_target="tpu_custom_call" | custom-call | tf_op jit(solution)/shard_map/layer/pallas_call | solution.py:635
  91.0 4.3 %store.1 = (bf16[160,1024]{1,0:T(8,128)(2,1)}, f32[512,512]{1,0:T(8,128)}, f32[512,256]{1,0:T(8,128)}, f32[512,256]{1,0:T(8,128)}, f32[512,512]{1,0:T(8,128)}, /*index=5*/f32[1,4]{1,0:T(1,128)}) custom-call(bf16[160,1024]{1,0:T(8,128)(2,1)} %get-tuple-element.18.refs_0_, f32[512,512]{1,0:T(8,128)} %get-tuple-element.19.refs_1_, ...), custom_call_target="tpu_custom_call" | custom-call | tf_op jit(solution)/shard_map/store/pallas_call | solution.py:681
